TPU v7x, 256 devices: a whole 4x4x8 slice. The times are simulated.
256 devices in a mesh: rep: 2 (over z_hi), fs: 16 (over z_lo, x), tp: 8 (over y, core).
Axes of the slice: x: 4, y: 4, z: 8 (z_hi: 2, z_lo: 4; z = z_hi * 4 + z_lo), core: 2. Of those that a mesh axis runs over, the one named last changes fastest.
Arguments:
- stream: bfloat16 [32768, 2048], P(('rep', 'fs', 'tp')), may hold values from -6 to 6
- gate_weight: bfloat16 [2048, 2816], P('fs', 'tp'), may hold values from -0.125 to 0.125
- up_weight: bfloat16 [2048, 2816], P('fs', 'tp'), may hold values from -0.125 to 0.125
- down_weight: bfloat16 [2816, 2048], P('tp', 'fs'), may hold values from -0.21875 to 0.21875
- query_weight: bfloat16 [2048, 512], P('fs', 'tp'), may hold values from -0.125 to 0.125
- key_weight: bfloat16 [2048, 512], P('fs', 'tp'), may hold values from -0.125 to 0.125
- value_weight: bfloat16 [2048, 1024], P('fs', 'tp'), may hold values from -0.125 to 0.125
- outgate_weight: bfloat16 [2048, 1024], P('fs', 'tp'), may hold values from -0.125 to 0.125
- decay_down: bfloat16 [2048, 32], replicated, may hold values from -0.125 to 0.125
- decay_up: bfloat16 [32, 512], P(None, 'tp'), may hold values from -2 to 2
- decay_bias: float32 [512], P('tp'), may hold values from -0.5 to 7
- head_gain: float32 [128], replicated, may hold values from 0.1 to 1.9
- out_weight: bfloat16 [1024, 2048], P('tp', 'fs'), may hold values from -0.375 to 0.375
- norm_gain: float32 [3, 2048], replicated, may hold values from 0.1 to 1.9
Outputs:
- layer_out: bfloat16 [32768, 2048], P(('rep', 'fs', 'tp'))
All inputs are finite; a program needn't handle non-finite values.
Results may differ from a plain program's by a relative error of at most 0.015.
Values may be sent and summed in bfloat16 or wider, within the bound.
A program may use at most 128 MiB of HBM per device.

v0:
```python
import jax
import jax.numpy as jnp
from jax import lax
from jax.sharding import PartitionSpec as P

DK = 64
DV = 128
BLOCK = 64
RESIDUAL_SCALE = 2.0**0.5
BRANCH_SCALE = 0.5
NORM_EPS = 1e-05
HEAD_EPS = 0.01
GATE_DIVISOR = 16.0


def from_everyone(value, axis):
    copies = jnp.broadcast_to(value, (lax.axis_size(axis), *value.shape))
    return lax.all_to_all(copies, axis, split_axis=0, concat_axis=0, tiled=True)


def joined_along(pieces, dim):
    pieces = jnp.moveaxis(pieces, 0, dim)
    lengths = pieces.shape
    return pieces.reshape(*lengths[:dim], lengths[dim] * lengths[dim + 1], *lengths[dim + 2 :])


def gather_directly(value, axis, dim):
    pieces = from_everyone(value, axis)
    return joined_along(pieces, dim)


def side_by_side(arrays, axis, dim, along):
    widths = [a.shape[along] for a in arrays]
    both = jnp.concatenate(arrays, axis=along)
    result = lax.all_gather(both, axis, axis=dim, tiled=True)
    return tuple(jnp.split(result, [sum(widths[:k]) for k in range(1, len(widths))], axis=along))


def layer_norm(values, norm_scale):
    average = jnp.mean(values, -1, keepdims=True)
    centred = values - average
    spread = jnp.mean(centred * centred, -1, keepdims=True)
    return (centred * lax.rsqrt(spread + NORM_EPS) * norm_scale).astype(jnp.bfloat16)


def blocked_mixer(query, key_rows, value_rows, log_gate):
    length, head_count, key_dim = query.shape
    value_dim = value_rows.shape[2]
    block_count = length // BLOCK

    def split_blocks(values):
        return values.reshape(block_count, BLOCK, head_count, values.shape[2]).transpose(0, 2, 1, 3)

    causal = jnp.tril(jnp.ones((BLOCK, BLOCK), dtype=bool))

    def advance(carried, inputs):
        query_blk, key_blk, value_blk, decay_blk = inputs
        log_gaps = decay_blk[:, :, None, :] - decay_blk[:, None, :, :]
        log_gaps = jnp.where(causal[None, :, :, None], log_gaps, -jnp.inf)
        scores = jnp.sum(
            query_blk[:, :, None, :] * key_blk[:, None, :, :] * jnp.exp(log_gaps), axis=-1
        )
        inside = jnp.einsum("hij,hjv->hiv", scores, value_blk)
        carried_part = jnp.einsum("hid,hdv->hiv", query_blk * jnp.exp(decay_blk), carried)
        closing = decay_blk[:, -1, :]
        update = jnp.einsum(
            "hjd,hjv->hdv", key_blk * jnp.exp(closing[:, None, :] - decay_blk), value_blk
        )
        return (carried * jnp.exp(closing)[:, :, None] + update, inside + carried_part)

    cumulative = jnp.cumsum(split_blocks(log_gate), axis=2)
    start_state = jnp.zeros((head_count, key_dim, value_dim), jnp.float32)
    _, outputs = lax.scan(
        advance,
        start_state,
        (split_blocks(query), split_blocks(key_rows), split_blocks(value_rows), cumulative),
    )
    return outputs.transpose(0, 2, 1, 3).reshape(length, head_count, value_dim)


def on_device(
    stream,
    gate_weight,
    up_weight,
    down_weight,
    query_weight,
    key_weight,
    value_weight,
    outgate_weight,
    decay_down,
    decay_up,
    decay_bias,
    head_gain,
    out_weight,
    norm_gain,
):
    down_local = gather_directly(down_weight, "fs", 1)
    down_full = lax.all_gather(down_local, "tp", axis=0, tiled=True)

    def ffn_half(current, norm_scale):
        gathered = lax.all_gather(current, "tp", axis=0, tiled=True)
        pieces = side_by_side((gate_weight, up_weight), "fs", 0, 1)
        gate = jnp.dot(gathered, pieces[0], preferred_element_type=jnp.float32)
        upward = jnp.dot(gathered, pieces[1], preferred_element_type=jnp.float32)
        hidden = (jax.nn.silu(gate) * upward).astype(jnp.bfloat16)
        own_hidden = lax.all_to_all(hidden, "tp", split_axis=0, concat_axis=1, tiled=True)
        summed = jnp.dot(own_hidden, down_full, preferred_element_type=jnp.float32)
        return layer_norm(
            RESIDUAL_SCALE * current.astype(jnp.float32) + BRANCH_SCALE * summed, norm_scale
        )

    first = ffn_half(stream, norm_gain[0])
    gathered = lax.all_gather(first, "tp", axis=0, tiled=True)
    length = gathered.shape[0]
    pieces = side_by_side((query_weight, key_weight, value_weight, outgate_weight), "fs", 0, 1)
    query, key_rows, value_rows, outgate = tuple(
        (jnp.dot(gathered, piece, preferred_element_type=jnp.float32) for piece in pieces)
    )
    query = query.astype(jnp.bfloat16)
    key_rows = key_rows.astype(jnp.bfloat16)
    value_rows = value_rows.astype(jnp.bfloat16)
    outgate = outgate.astype(jnp.bfloat16)
    low_rank = jnp.dot(gathered, decay_down, preferred_element_type=jnp.float32).astype(
        jnp.bfloat16
    )
    pre_gate = jnp.dot(low_rank, decay_up, preferred_element_type=jnp.float32) + decay_bias
    log_gate = jax.nn.log_sigmoid(pre_gate) / GATE_DIVISOR
    local_heads = query.shape[1] // DK
    mixed = blocked_mixer(
        query.astype(jnp.float32).reshape(length, local_heads, DK) * DK ** (-0.5),
        key_rows.astype(jnp.float32).reshape(length, local_heads, DK),
        value_rows.astype(jnp.float32).reshape(length, local_heads, DV),
        log_gate.reshape(length, local_heads, DK),
    )
    normed = mixed * lax.rsqrt(jnp.mean(mixed * mixed, -1, keepdims=True) + HEAD_EPS) * head_gain
    gated = (
        normed.reshape(length, local_heads * DV) * jax.nn.silu(outgate.astype(jnp.float32))
    ).astype(jnp.bfloat16)
    out_local = gather_directly(out_weight, "fs", 1)
    out_full = lax.all_gather(out_local, "tp", axis=0, tiled=True)
    own_gated = lax.all_to_all(gated, "tp", split_axis=0, concat_axis=1, tiled=True)
    summed = jnp.dot(own_gated, out_full, preferred_element_type=jnp.float32)
    second = layer_norm(RESIDUAL_SCALE * first.astype(jnp.float32) + summed, norm_gain[1])
    return ffn_half(second, norm_gain[2])


def solution(mesh):
    in_specs = (
        P(("rep", "fs", "tp"), None),
        P("fs", "tp"),
        P("fs", "tp"),
        P("tp", "fs"),
        P("fs", "tp"),
        P("fs", "tp"),
        P("fs", "tp"),
        P("fs", "tp"),
        P(),
        P(None, "tp"),
        P("tp"),
        P(),
        P("tp", "fs"),
        P(),
    )
    out_specs = P(("rep", "fs", "tp"), None)
    return jax.shard_map(
        on_device, mesh=mesh, in_specs=in_specs, out_specs=out_specs, check_vma=False
    )
```

profile of v0, /device:TPU:1, one launch (start us, length us, event | category | flops | bytes accessed | tf_op | source)
XLA Modules:
  0.0 473.2 jit_solution(7399616951409170826)
XLA Ops:
  6.5 1.7 pad_maximum_fusion
  8.3 0.7 all-gather.10.cloned.1.call-update
  9.0 1.1 broadcast_in_dim.32
  10.1 57.1 %all_to_all.67 = bf16[16,352,128]{2,1,0:T(8,128)(2,1)S(1)} all-to-all(bf16[16,352,128]{2,1,0:T(8,128)(2,1)S(1)} %broadcast_in_dim.32), channel_id=1, replica_groups=mesh['rep'=2,'fs'=16,'tp'=8] {'fs'}, dimensions={0} | all-to-all | bytes 2883584 | tf_op jit(solution)/shard_map/all_to_all | solution.py:18
  67.2 1.3 copy_bitcast_fusion
  68.9 0.7 pad_maximum_fusion.1
  69.6 27.4 %all-gather.8.cloned.1.call-done = bf16[2048,704]{0,1:T(8,128)(2,1)} async-done(((bf16[128,704]{0,1:T(8,128)(2,1)}), bf16[2048,704]{0,1:T(8,128)(2,1)}) %all-gather.8.cloned.1.call-update) | async-done | bytes 2883600 | tf_op jit(solution)/shard_map/all_gather | solution.py:35
  97.0 44.9 %all-gather.10.cloned.1.call-done = bf16[1024,2048]{1,0:T(8,128)(2,1)} async-done(((bf16[128,2048]{1,0:T(8,128)(2,1)}), bf16[1024,2048]{1,0:T(8,128)(2,1)}) %all-gather.10.cloned.1.call-update) | async-done | bytes 4194320 | tf_op jit(solution)/shard_map/all_gather | solution.py:101
  141.9 4.5 convolution_bitcast_fusion.2
  146.4 1.9 fusion.35
  148.3 1.0 copy.67
  149.3 3.7 all-to-all-start
  153.1 14.9 %all-to-all-done = bf16[8,128,352]{1,2,0:T(8,128)(2,1)S(1)} async-done(((bf16[8,128,352]{1,2,0:T(8,128)(2,1)}), bf16[8,128,352]{1,2,0:T(8,128)(2,1)S(1)}, u32[]{:S(2)}, u32[]{:S(2)}) %all-to-all-start) | async-done | bytes 720928 | tf_op jit(solution)/shard_map/all_to_all | solution.py:106
  168.0 45.3 %all-gather.12.cloned.1.call-done = bf16[2816,2048]{1,0:T(8,128)(2,1)} async-done(((bf16[352,2048]{1,0:T(8,128)(2,1)}), bf16[2816,2048]{1,0:T(8,128)(2,1)}) %all-gather.12.cloned.1.call-update) | async-done | bytes 11534352 | tf_op jit(solution)/shard_map/all_gather | solution.py:98
  213.3 6.0 %fusion.58 = (f32[128]{0:T(128)S(1)}, f32[128,2048]{1,0:T(8,128)S(1)}) fusion(bf16[128,2816]{0,1:T(8,128)(2,1)S(1)} %bitcast.148, bf16[2816,2048]{1,0:T(8,128)(2,1)} %all-gather.12.cloned.1.call-done, bf16[128,2048]{1,0:T(8,128)(2,1)S(1)} %copy-done.3), kind=kOutput, calls=%fused_computation.96 | convolution fusion | flops 1477705600 | bytes 13828608 | tf_op jit(solution)/shard_map/dot_general | solution.py:107
  219.3 0.3 multiply_reduce_fusion.3
  219.6 1.0 multiply_convert_fusion.2
  220.8 0.9 broadcast_in_dim.35
  221.7 7.0 %all-to-all-start.3 = ((bf16[16,128,128]{1,2,0:T(8,128)(2,1)}), bf16[16,128,128]{1,2,0:T(8,128)(2,1)S(1)}, u32[]{:S(2)}, u32[]{:S(2)}) async-start(bf16[16,128,128]{1,2,0:T(8,128)(2,1)} %broadcast_in_dim.35), calls=%async_computation.3 | async-start | bytes 1048576 | tf_op jit(solution)/shard_map/all_to_all | solution.py:18
  228.8 0.2 all-gather.18.cloned.1.call-start
  229.0 17.3 %all-to-all-done.3 = bf16[16,128,128]{1,2,0:T(8,128)(2,1)S(1)} async-done(((bf16[16,128,128]{1,2,0:T(8,128)(2,1)}), bf16[16,128,128]{1,2,0:T(8,128)(2,1)S(1)}, u32[]{:S(2)}, u32[]{:S(2)}) %all-to-all-start.3) | async-done | bytes 524320 | tf_op jit(solution)/shard_map/all_to_all | solution.py:18
  246.3 0.9 copy-done.4
  247.2 39.2 %all-gather.16.cloned.1.call-done = bf16[2048,384]{1,0:T(8,128)(2,1)} async-done(((bf16[128,384]{1,0:T(8,128)(2,1)}), bf16[2048,384]{1,0:T(8,128)(2,1)}) %all-gather.16.cloned.1.call-update) | async-done | bytes 1572880 | tf_op jit(solution)/shard_map/all_gather | solution.py:35
  286.4 45.3 %all-gather.14.cloned.1.call-done = bf16[1024,2048]{1,0:T(8,128)(2,1)} async-done(((bf16[128,2048]{1,0:T(8,128)(2,1)}), bf16[1024,2048]{1,0:T(8,128)(2,1)}) %all-gather.14.cloned.1.call-update) | async-done | bytes 4194320 | tf_op jit(solution)/shard_map/all_gather | solution.py:113
  331.8 3.8 fusion.45
  335.5 0.2 copy.57
  335.7 3.7 fusion.44
  339.5 0.2 copy.58
  339.7 3.8 fusion.56
  343.6 0.4 copy.47
  344.0 6.3 %fusion.61 = f32[16,1,64,64]{3,0,1,2:T(8,128)S(1)} fusion(f32[16,1,64,64]{3,0,1,2:T(8,128)S(1)} %copy.47), kind=kOutput, calls=%fused_computation.99 | output fusion | flops 4128768 | bytes 524288 | tf_op jit(solution)/shard_map/jit(cumsum)/reduce_window_sum | solution.py:71
  350.3 3.6 convolution_convert_fusion.1
  353.9 30.5 %while.13 = (s32[]{:T(128)}, f32[1,64,128]{2,1,0:T(8,128)S(1)}, f32[16,1,64,128]{3,2,1,0:T(8,128)S(1)}, f32[16,1,64,64]{3,0,1,2:T(8,128)S(1)}, f32[16,1,64,64]{3...) while((s32[]{:T(128)}, f32[1,64,128]{2,1,0:T(8,128)S(1)}, ...), condition=%wide.region_5.6_spmd.clone, body=%wide.region_3.5_spmd.clone.sunk | while | flops 4509699 | bytes 544884 | solution.py:73
  354.0 1.4 multiply_reduce_fusion.6
  355.9 1.4 multiply_reduce_fusion.6
  357.8 1.4 multiply_reduce_fusion.6
  359.7 1.4 multiply_reduce_fusion.6
  361.6 1.4 multiply_reduce_fusion.6
  363.5 1.4 multiply_reduce_fusion.6
  365.4 1.4 multiply_reduce_fusion.6
  367.3 1.4 multiply_reduce_fusion.6
  369.2 1.4 multiply_reduce_fusion.6
  371.1 1.4 multiply_reduce_fusion.6
  373.0 1.4 multiply_reduce_fusion.6
  374.9 1.4 multiply_reduce_fusion.6
  376.8 1.4 multiply_reduce_fusion.6
  378.7 1.4 multiply_reduce_fusion.6
  380.6 1.4 multiply_reduce_fusion.6
  382.6 1.4 multiply_reduce_fusion.6
  384.4 0.2 multiply_reduce_fusion.4
  384.7 3.6 fusion.52
  388.3 0.9 copy.54
  389.2 3.6 all-to-all-start.2
  392.8 6.5 %all-to-all-done.2 = bf16[8,128,128]{1,2,0:T(8,128)(2,1)S(1)} async-done(((bf16[8,128,128]{1,2,0:T(8,128)(2,1)}), bf16[8,128,128]{1,2,0:T(8,128)(2,1)S(1)}, u32[]{:S(2)}, u32[]{:S(2)}) %all-to-all-start.2) | async-done | bytes 262176 | tf_op jit(solution)/shard_map/all_to_all | solution.py:141
  399.3 3.8 fusion.59
  403.0 0.3 multiply_reduce_fusion.2
  403.3 1.0 multiply_convert_fusion.1
  404.4 35.0 %all-gather.20.cloned.1.call-done = bf16[1024,2048]{1,0:T(8,128)(2,1)} async-done(((bf16[128,2048]{1,0:T(8,128)(2,1)}), bf16[1024,2048]{1,0:T(8,128)(2,1)}) %all-gather.20.cloned.1.call-update) | async-done | bytes 4194320 | tf_op jit(solution)/shard_map/all_gather | solution.py:101
  439.3 4.5 fusion.38
  443.8 4.6 fusion.34
  448.6 14.7 %all_to_all.68 = bf16[8,128,352]{1,2,0:T(8,128)(2,1)S(1)} all-to-all(bf16[8,128,352]{1,2,0:T(8,128)(2,1)S(1)} %bitcast.150), channel_id=1, replica_groups=mesh['rep'=2,'fs'=16,'tp'=8] {'tp'}, dimensions={0} | all-to-all | bytes 1441792 | tf_op jit(solution)/shard_map/all_to_all | solution.py:106
  463.3 1.8 fusion.60
  465.1 0.3 multiply_reduce_fusion.1
  465.3 1.0 multiply_convert_fusion
  (195 shorter events, 9.2 us)
Async XLA Ops:
  6.5 333.1 %copy-start = (bf16[2048,32]{0,1:T(8,128)(2,1)S(1)}, bf16[2048,32]{0,1:T(8,128)(2,1)}, u32[]{:S(2)}) copy-start(bf16[2048,32]{0,1:T(8,128)(2,1)} %param.24) | copy-start | bytes 393220
  6.5 90.5 %all-gather.8.cloned.1.call-start = ((), (), s32[]{:S(2)}) async-start(), calls=%async_computation.5 | async-start | bytes 3063808 | tf_op jit(solution)/shard_map/all_gather | solution.py:35
  8.2 133.7 %all-gather.10.cloned.1.call-start = ((), (), s32[]{:S(2)}) async-start(), calls=%async_computation.6 | async-start | bytes 4718592 | tf_op jit(solution)/shard_map/all_gather | solution.py:101
  9.0 204.3 %all-gather.12.cloned.1.call-start = ((), (), s32[]{:S(2)}) async-start(), calls=%async_computation.7 | async-start | bytes 12976128 | tf_op jit(solution)/shard_map/all_gather | solution.py:98
  67.2 1.4 copy-start.9
  67.2 1.5 copy-start.10
  67.2 1.6 copy-start.5
  67.2 1.6 copy-start.6
  68.6 217.8 %all-gather.16.cloned.1.call-start = ((), (), s32[]{:S(2)}) async-start(), calls=%async_computation.9 | async-start | bytes 1671168 | tf_op jit(solution)/shard_map/all_gather | solution.py:35
  97.0 49.4 %copy-start.14 = (bf16[2048,704]{0,1:T(8,128)(2,1)S(1)}, bf16[2048,704]{0,1:T(8,128)(2,1)}, u32[]{:S(2)}) copy-start(bf16[2048,704]{0,1:T(8,128)(2,1)} %all-gather.8.cloned.1.call-done) | copy-start | bytes 8650756
  141.9 4.5 copy-start.13
  148.3 4.8 %copy-start.8 = (f32[3,2048]{1,0:T(4,128)S(1)}, f32[3,2048]{1,0:T(4,128)}, u32[]{:S(2)}) copy-start(f32[3,2048]{1,0:T(4,128)} %param.29) | copy-start | bytes 73732
  148.3 64.9 %copy-start.3 = (bf16[128,2048]{1,0:T(8,128)(2,1)S(1)}, bf16[128,2048]{1,0:T(8,128)(2,1)}, u32[]{:S(2)}) copy-start(bf16[128,2048]{1,0:T(8,128)(2,1)} %param.16) | copy-start | bytes 1572868
  149.3 18.6 %all-to-all-start = ((bf16[8,128,352]{1,2,0:T(8,128)(2,1)}), bf16[8,128,352]{1,2,0:T(8,128)(2,1)S(1)}, u32[]{:S(2)}, u32[]{:S(2)}) async-start(bf16[8,128,352]{1,2,0:T(8,128)(2,1)} %bitcast.112), calls=%async_computation | async-start | bytes 1441792 | tf_op jit(solution)/shard_map/all_to_all | solution.py:106
  153.1 178.7 %all-gather.14.cloned.1.call-start = ((), (), s32[]{:S(2)}) async-start(), calls=%async_computation.8 | async-start | bytes 4718592 | tf_op jit(solution)/shard_map/all_gather | solution.py:113
  219.3 1.3 copy-start.7
  221.7 24.6 %all-to-all-start.3 = ((bf16[16,128,128]{1,2,0:T(8,128)(2,1)}), bf16[16,128,128]{1,2,0:T(8,128)(2,1)S(1)}, u32[]{:S(2)}, u32[]{:S(2)}) async-start(bf16[16,128,128]{1,2,0:T(8,128)(2,1)} %broadcast_in_dim.35), calls=%async_computation.3 | async-start | bytes 1048576 | tf_op jit(solution)/shard_map/all_to_all | solution.py:18
  228.8 164.0 %all-gather.18.cloned.1.call-start = ((), (), s32[]{:S(2)}) async-start(), calls=%async_computation.10 | async-start | bytes 4718592 | tf_op jit(solution)/shard_map/all_gather | solution.py:140
  246.3 0.9 copy-start.4
  335.7 4.0 copy-start.11
  335.7 4.0 copy-start.12
  353.9 30.8 %copy-start.15 = (f32[128]{0:T(128)S(1)}, f32[128]{0:T(128)}, u32[]{:S(2)}) copy-start(f32[128]{0:T(128)} %param.27) | copy-start | bytes 1540
  384.7 14.6 %copy-start.1 = (bf16[128,2048]{1,0:T(8,128)(2,1)S(1)}, bf16[128,2048]{1,0:T(8,128)(2,1)}, u32[]{:S(2)}) copy-start(bf16[128,2048]{1,0:T(8,128)(2,1)} %multiply_convert_fusion.2) | copy-start | bytes 1572868
  389.2 10.1 %all-to-all-start.2 = ((bf16[8,128,128]{1,2,0:T(8,128)(2,1)}), bf16[8,128,128]{1,2,0:T(8,128)(2,1)S(1)}, u32[]{:S(2)}, u32[]{:S(2)}) async-start(bf16[8,128,128]{1,2,0:T(8,128)(2,1)} %copy.54), calls=%async_computation.2 | async-start | bytes 524288 | tf_op jit(solution)/shard_map/all_to_all | solution.py:141
  392.8 46.6 %all-gather.20.cloned.1.call-start = ((), (), s32[]{:S(2)}) async-start(), calls=%async_computation.11 | async-start | bytes 4718592 | tf_op jit(solution)/shard_map/all_gather | solution.py:101
  439.3 23.9 %slice-start = ((s8[11534336]{0:T(1024)(128)(4,1)}), s8[4194304]{0:T(1024)(128)(4,1)S(1)}, s32[]{:S(2)}) async-start(s8[11534336]{0:T(1024)(128)(4,1)} %bitcast.141), calls=%async_computation.12 | async-start | bytes 8388608
  439.3 23.9 %slice-start.1 = ((s8[11534336]{0:T(1024)(128)(4,1)}), s8[4194304]{0:T(1024)(128)(4,1)S(1)}, s32[]{:S(2)}) async-start(s8[11534336]{0:T(1024)(128)(4,1)} %bitcast.141), calls=%async_computation.13 | async-start | bytes 8388608
  443.8 19.5 %slice-start.2 = ((s8[11534336]{0:T(1024)(128)(4,1)}), s8[3145728]{0:T(1024)(128)(4,1)S(1)}, s32[]{:S(2)}) async-start(s8[11534336]{0:T(1024)(128)(4,1)} %bitcast.141), calls=%async_computation.14 | async-start | bytes 6291456
  448.4 14.8 %copy-start.2 = (bf16[128,2048]{1,0:T(8,128)(2,1)S(1)}, bf16[128,2048]{1,0:T(8,128)(2,1)}, u32[]{:S(2)}) copy-start(bf16[128,2048]{1,0:T(8,128)(2,1)} %multiply_convert_fusion.1) | copy-start | bytes 1572868
Sparse Core Ops, SparseCore 0:
  9.0 87.9 all-gather.7
  98.9 42.9 all-gather.9
  143.8 69.4 all-gather.11
  214.9 71.4 all-gather.15
  288.1 43.5 all-gather.13
  333.4 38.1 all-gather.17
  404.5 34.8 all-gather.19
where the time goes:
time: 474 us; the launch traced here: 473 us
  waiting for transfers between devices  277 us (58%)
  blocking collectives  71.8 us (15%)
  matrix products  52.6 us (11%)
  other arithmetic  34.7 us (7%)
  starting transfers between devices  14.7 us (3%)
  between operations  13.8 us (3%)
  local copies, waits for them, and re-layouts  8.37 us (2%)
    all_gather x2, waiting for transfers between devices, ffn_half(): gathered = lax.all_gather(current, 'tp', axis=0, tiled=True)  79.9 us
    all_gather x2, waiting for transfers between devices, side_by_side(): result = lax.all_gather(both, axis, axis=dim, tiled=True)  66.6 us
    all_to_all x1, blocking collectives, from_everyone(): return lax.all_to_all(copies, axis, split_axis=0, concat_axis=0, tiled=True)  57.1 us
    all_gather x1, waiting for transfers between devices, on_device(): gathered = lax.all_gather(first, 'tp', axis=0, tiled=True)  45.3 us
    all_gather x1, waiting for transfers between devices, on_device(): down_full = lax.all_gather(down_local, 'tp', axis=0, tiled=True)  45.3 us
    reduce_sum x16, other arithmetic, advance(): jnp.sum(query_blk[:, :, None, :] * key_blk[:, None, :, :] * jnp.exp(log_g...  21.7 us
    all_to_all x1, waiting for transfers between devices, from_everyone(): return lax.all_to_all(copies, axis, split_axis=0, concat_axis=0, tiled=True)  17.3 us
    all_to_all x1, waiting for transfers between devices, ffn_half(): lax.all_to_all(hidden, 'tp', split_axis=0, concat_axis=1, tiled=True)  14.9 us
  transfers between devices with their start and end apart: 10, of which 9 were waited for; matrix products, arithmetic and copies ran while one was open for 16% of the time, Pallas kernels for 0%

commit v1 on v0

--- a/solution.py
+++ b/solution.py
@@ -11,6 +11,28 @@
 NORM_EPS = 1e-05
 HEAD_EPS = 0.01
 GATE_DIVISOR = 16.0
+
+
+def in_order(blocks, dim):
+    blocks = jnp.moveaxis(blocks, 0, dim)
+    shape = blocks.shape
+    return blocks.reshape(*shape[:dim], shape[dim] * shape[dim + 1], *shape[dim + 2 :])
+
+
+def ring_gather(shard, axis, dim):
+    size = lax.axis_size(axis)
+    pairs = [(i, (i + 1) % size) for i in range(size)]
+    back = [(b, a) for a, b in pairs]
+    lower, upper = ([], [])
+    for step in range(size - 1):
+        if step % 2 == 0:
+            lower.append(lax.ppermute(lower[-1] if lower else shard, axis, pairs))
+        else:
+            upper.append(lax.ppermute(upper[-1] if upper else shard, axis, back))
+    tiles = jnp.stack([*lower[::-1], shard, *upper])
+    shift = lax.axis_index(axis) - len(lower)
+    tiles = tiles[(jnp.arange(size) - shift) % size]
+    return in_order(tiles, dim)
 
 
 def from_everyone(value, axis):
@@ -95,7 +117,7 @@
     norm_gain,
 ):
     down_local = gather_directly(down_weight, "fs", 1)
-    down_full = lax.all_gather(down_local, "tp", axis=0, tiled=True)
+    down_full = ring_gather(down_local, "tp", 0)
 
     def ffn_half(current, norm_scale):
         gathered = lax.all_gather(current, "tp", axis=0, tiled=True)

time: 474 us -> 447 us (0.943)
  blocking collectives: 71.8 us -> 14.7 us
  waiting for transfers between devices: 277 us -> 229 us
  starting transfers between devices: 14.7 us -> 61.9 us
  local copies, waits for them, and re-layouts: 8.37 us -> 39.6 us
    all_to_all x1 -> x0, blocking collectives: 57.1 us -> none  [from_everyone(): return lax.all_to_all(copies, axis, split_axis=0, concat_axis=0, tiled=True)]
    ppermute x0 -> x7, waiting for transfers between devices: none -> 46.6 us  [the longest x4 46.6 us: ring_gather(): lower.append(lax.ppermute(lower[-1] if lower else shard, axis, pairs))]
    all_gather x1 -> x0, waiting for transfers between devices: 45.3 us -> none  [on_device(): down_full = lax.all_gather(down_local, 'tp', axis=0, tiled=True)]
    all_to_all x1 -> x2, waiting for transfers between devices: 17.3 us -> 51.4 us  [from_everyone(): return lax.all_to_all(copies, axis, split_axis=0, concat_axis=0, tiled=True)]
    all_gather x1, waiting for transfers between devices: 45.3 us -> 12.7 us  [on_device(): gathered = lax.all_gather(first, 'tp', axis=0, tiled=True)]
    all_gather x2, waiting for transfers between devices: 79.9 us -> 49.6 us  [ffn_half(): gathered = lax.all_gather(current, 'tp', axis=0, tiled=True)]
    ppermute x0 -> x7, starting transfers between devices: none -> 24.6 us  [the longest x4 15.6 us: ring_gather(): lower.append(lax.ppermute(lower[-1] if lower else shard, axis, pairs))]
    unnamed x43 -> x62, local copies, waits for them, and re-layouts: 1.67 us -> 18.6 us
  transfers between devices with their start and end apart: 10 -> 17, of which waited for: 9 -> 10; matrix products, arithmetic and copies ran while one was open for 16% -> 22% of each run, Pallas kernels for 0% -> 0%
where the time goes in v1:
time: 447 us; the launch traced here: 446 us
  waiting for transfers between devices  229 us (51%)
  starting transfers between devices  61.9 us (14%)
  matrix products  51.7 us (12%)
  local copies, waits for them, and re-layouts  39.6 us (9%)
  other arithmetic  34.7 us (8%)
  blocking collectives  14.7 us (3%)
  between operations  13.9 us (3%)
    all_gather x2, waiting for transfers between devices, side_by_side(): result = lax.all_gather(both, axis, axis=dim, tiled=True)  61.6 us
    all_to_all x2, waiting for transfers between devices, from_everyone(): return lax.all_to_all(copies, axis, split_axis=0, concat_axis=0, tiled=True)  51.4 us
    all_gather x2, waiting for transfers between devices, ffn_half(): gathered = lax.all_gather(current, 'tp', axis=0, tiled=True)  49.6 us
    ppermute x4, waiting for transfers between devices, ring_gather(): lower.append(lax.ppermute(lower[-1] if lower else shard, axis, pairs))  46.6 us
    reduce_sum x16, other arithmetic, advance(): jnp.sum(query_blk[:, :, None, :] * key_blk[:, None, :, :] * jnp.exp(log_g...  21.7 us
    unnamed x62, local copies, waits for them, and re-layouts  18.6 us
    all_to_all x2, starting transfers between devices, from_everyone(): return lax.all_to_all(copies, axis, split_axis=0, concat_axis=0, tiled=True)  17.5 us
    all_to_all x1, starting transfers between devices, on_device(): lax.all_to_all(gated, 'tp', split_axis=0, concat_axis=1, tiled=True)  15.8 us
  transfers between devices with their start and end apart: 17, of which 10 were waited for; matrix products, arithmetic and copies ran while one was open for 22% of the time, Pallas kernels for 0%

profile of v1, /device:TPU:1, one launch (start us, length us, event | category | flops | bytes accessed | tf_op | source)
XLA Modules:
  0.0 446.2 jit_solution(5728296789005256240)
XLA Ops:
  6.5 1.7 pad_maximum_fusion
  8.2 2.2 broadcast_in_dim.32
  10.4 9.1 %all-to-all-start.1 = ((bf16[16,352,128]{2,1,0:T(8,128)(2,1)}), bf16[16,352,128]{2,1,0:T(8,128)(2,1)S(1)}, u32[]{:S(2)}, u32[]{:S(2)}) async-start(bf16[16,352,128]{2,1,0:T(8,128)(2,1)} %broadcast_in_dim.32), calls=%async_computation.1 | async-start | bytes 2883584 | tf_op jit(solution)/shard_map/all_to_all | solution.py:40
  20.3 37.4 %all-to-all-done.1 = bf16[16,352,128]{2,1,0:T(8,128)(2,1)S(1)} async-done(((bf16[16,352,128]{2,1,0:T(8,128)(2,1)}), bf16[16,352,128]{2,1,0:T(8,128)(2,1)S(1)}, u32[]{:S(2)}, u32[]{:S(2)}) %all-to-all-start.1) | async-done | bytes 1441824 | tf_op jit(solution)/shard_map/all_to_all | solution.py:40
  57.9 8.0 %collective-permute-start = (bf16[352,2048]{1,0:T(8,128)(2,1)S(1)}, bf16[352,2048]{1,0:T(8,128)(2,1)S(1)}, u32[]{:S(2)}, u32[]{:S(2)}) collective-permute-start(bf16[352,2048]{1,0:T(8,128)(2,1)S(1)} %copy_bitcast_fusion), channel_id=1, source_target_pairs={{0,1},{1,2},{2,3},{3,4},{4,5},{5,6},{6,7},{7,0},{8,9},{9,10},{10,1... | collective-permute-start | bytes 4325384 | tf_op jit(solution)/shard_map/ppermute | solution.py:29
  66.0 16.0 %collective-permute-done = bf16[352,2048]{1,0:T(8,128)(2,1)S(1)} collective-permute-done((bf16[352,2048]{1,0:T(8,128)(2,1)S(1)}, bf16[352,2048]{1,0:T(8,128)(2,1)S(1)}, u32[]{:S(2)}, u32[]{:S(2)}) %collective-permute-start) | collective-permute-done | bytes 1441824 | tf_op jit(solution)/shard_map/ppermute | solution.py:29
  81.9 1.1 copy-done.6
  83.0 2.5 collective-permute-start.1
  85.5 15.9 %collective-permute-done.1 = bf16[352,2048]{1,0:T(8,128)(2,1)S(1)} collective-permute-done((bf16[352,2048]{1,0:T(8,128)(2,1)S(1)}, bf16[352,2048]{1,0:T(8,128)(2,1)S(1)}, u32[]{:S(2)}, u32[]{:S(2)}) %collective-permute-start.1) | collective-permute-done | bytes 1441824 | tf_op jit(solution)/shard_map/ppermute | solution.py:29
  101.5 1.1 copy-done.8
  102.6 2.5 collective-permute-start.2
  105.0 1.2 collective-permute-start.5
  106.3 14.7 %collective-permute-done.2 = bf16[352,2048]{1,0:T(8,128)(2,1)} collective-permute-done((bf16[352,2048]{1,0:T(8,128)(2,1)S(1)}, bf16[352,2048]{1,0:T(8,128)(2,1)}, u32[]{:S(2)}, u32[]{:S(2)}) %collective-permute-start.2) | collective-permute-done | bytes 1441824 | tf_op jit(solution)/shard_map/ppermute | solution.py:29
  121.0 2.6 collective-permute-start.3
  124.9 7.8 %collective-permute-start.6 = (bf16[352,2048]{1,0:T(8,128)(2,1)}, bf16[352,2048]{1,0:T(8,128)(2,1)}, u32[]{:S(2)}, u32[]{:S(2)}) collective-permute-start(bf16[352,2048]{1,0:T(8,128)(2,1)} %collective-permute-done.5), channel_id=1, source_target_pairs={{1,0},{2,1},{3,2},{4,3},{5,4},{6,5},{7,6},{0,7},{9,8},{10,9},{11,1... | collective-permute-start | bytes 4325384 | tf_op jit(solution)/shard_map/ppermute | solution.py:31
  132.6 17.4 %all-gather.9.cloned.1.call-done = bf16[1024,2048]{1,0:T(8,128)(2,1)} async-done(((bf16[128,2048]{1,0:T(8,128)(2,1)}), bf16[1024,2048]{1,0:T(8,128)(2,1)}) %all-gather.9.cloned.1.call-update) | async-done | bytes 4194320 | tf_op jit(solution)/shard_map/all_gather | solution.py:123
  150.0 4.5 convolution_bitcast_fusion.4
  154.8 1.8 fusion.37
  157.7 3.7 all-to-all-start
  161.4 2.8 bitcast_dynamic-update-slice_fusion.6
  164.2 2.7 bitcast_dynamic-update-slice_fusion.5
  166.9 1.2 bitcast_dynamic-update-slice_fusion.4
  168.2 1.2 bitcast_dynamic-update-slice_fusion.3
  169.4 1.2 constant_dynamic-update-slice_fusion
  170.6 2.6 bitcast_dynamic-update-slice_fusion.2
  173.2 2.6 bitcast_dynamic-update-slice_fusion.1
  175.9 2.7 bitcast_dynamic-update-slice_fusion
  178.5 10.4 %gather_fusion = bf16[8,352,2048]{2,1,0:T(8,128)(2,1)} fusion(bf16[8,352,2048]{2,1,0:T(8,128)(2,1)} %bitcast_dynamic-update-slice_fusion, s32[1024]{0:T(1024)S(1)} %pad_clamp_fusion), kind=kCustom, calls=%fused_computation | custom fusion | bytes 23068704 | tf_op jit(solution)/shard_map/gather | solution.py:34
  188.9 6.0 %fusion.64 = (f32[128]{0:T(128)S(1)}, f32[128,2048]{1,0:T(8,128)S(1)}) fusion(bf16[8,352,2048]{2,1,0:T(8,128)(2,1)} %gather_fusion, bf16[8,128,352]{1,2,0:T(8,128)(2,1)S(1)} %all-to-all-done, bf16[128,2048]{1,0:T(8,128)(2,1)S(1)} %copy-done.5), kind=kOutput, calls=%fused_computation.116 | convolution fusion | flops 1477705600 | bytes 13828608 | tf_op jit(solution)/shard_map/dot_general | solution.py:129
  198.5 8.4 %all-to-all-start.3 = ((bf16[16,128,128]{1,2,0:T(8,128)(2,1)}), bf16[16,128,128]{1,2,0:T(8,128)(2,1)S(1)}, u32[]{:S(2)}, u32[]{:S(2)}) async-start(bf16[16,128,128]{1,2,0:T(8,128)(2,1)} %broadcast_in_dim.35), calls=%async_computation.3 | async-start | bytes 1048576 | tf_op jit(solution)/shard_map/all_to_all | solution.py:40
  207.1 14.0 %all-to-all-done.3 = bf16[16,128,128]{1,2,0:T(8,128)(2,1)S(1)} async-done(((bf16[16,128,128]{1,2,0:T(8,128)(2,1)}), bf16[16,128,128]{1,2,0:T(8,128)(2,1)S(1)}, u32[]{:S(2)}, u32[]{:S(2)}) %all-to-all-start.3) | async-done | bytes 524320 | tf_op jit(solution)/shard_map/all_to_all | solution.py:40
  222.0 12.7 %all-gather.11.cloned.1.call-done = bf16[1024,2048]{1,0:T(8,128)(2,1)} async-done(((bf16[128,2048]{1,0:T(8,128)(2,1)}), bf16[1024,2048]{1,0:T(8,128)(2,1)}) %all-gather.11.cloned.1.call-update) | async-done | bytes 4194320 | tf_op jit(solution)/shard_map/all_gather | solution.py:135
  234.7 3.8 fusion.60
  239.0 6.3 %fusion.67 = f32[16,1,64,64]{3,0,1,2:T(8,128)S(1)} fusion(f32[16,1,64,64]{3,0,1,2:T(8,128)S(1)} %copy.51), kind=kOutput, calls=%fused_computation.119 | output fusion | flops 4128768 | bytes 524288 | tf_op jit(solution)/shard_map/jit(cumsum)/reduce_window_sum | solution.py:93
  245.3 61.6 %all-gather.13.cloned.1.call-done = bf16[2048,384]{1,0:T(8,128)(2,1)} async-done(((bf16[128,384]{1,0:T(8,128)(2,1)}), bf16[2048,384]{1,0:T(8,128)(2,1)}) %all-gather.13.cloned.1.call-update) | async-done | bytes 1572880 | tf_op jit(solution)/shard_map/all_gather | solution.py:57
  306.9 3.8 fusion.47
  310.9 3.7 fusion.46
  314.8 3.6 convolution_convert_fusion.1
  318.4 30.5 %while.13 = (s32[]{:T(128)}, f32[1,64,128]{2,1,0:T(8,128)S(1)}, f32[16,1,64,128]{3,2,1,0:T(8,128)S(1)}, f32[16,1,64,64]{3,0,1,2:T(8,128)S(1)}, f32[16,1,64,64]{3...) while((s32[]{:T(128)}, f32[1,64,128]{2,1,0:T(8,128)S(1)}, ...), condition=%wide.region_5.6_spmd.clone, body=%wide.region_3.5_spmd.clone.sunk | while | flops 4509699 | bytes 544884 | solution.py:95
  318.4 1.4 multiply_reduce_fusion.6
  320.3 1.4 multiply_reduce_fusion.6
  322.3 1.4 multiply_reduce_fusion.6
  324.2 1.4 multiply_reduce_fusion.6
  326.1 1.4 multiply_reduce_fusion.6
  328.0 1.4 multiply_reduce_fusion.6
  329.9 1.4 multiply_reduce_fusion.6
  331.8 1.4 multiply_reduce_fusion.6
  333.7 1.4 multiply_reduce_fusion.6
  335.6 1.4 multiply_reduce_fusion.6
  337.5 1.4 multiply_reduce_fusion.6
  339.4 1.4 multiply_reduce_fusion.6
  341.3 1.4 multiply_reduce_fusion.6
  343.2 1.4 multiply_reduce_fusion.6
  345.1 1.4 multiply_reduce_fusion.6
  347.0 1.4 multiply_reduce_fusion.6
  349.2 3.6 fusion.56
  353.7 15.8 %all-to-all-start.2 = ((bf16[8,128,128]{1,2,0:T(8,128)(2,1)}), bf16[8,128,128]{1,2,0:T(8,128)(2,1)S(1)}, u32[]{:S(2)}, u32[]{:S(2)}) async-start(bf16[8,128,128]{1,2,0:T(8,128)(2,1)} %copy.58), calls=%async_computation.2 | async-start | bytes 524288 | tf_op jit(solution)/shard_map/all_to_all | solution.py:163
  369.4 6.5 %all-to-all-done.2 = bf16[8,128,128]{1,2,0:T(8,128)(2,1)S(1)} async-done(((bf16[8,128,128]{1,2,0:T(8,128)(2,1)}), bf16[8,128,128]{1,2,0:T(8,128)(2,1)S(1)}, u32[]{:S(2)}, u32[]{:S(2)}) %all-to-all-start.2) | async-done | bytes 262176 | tf_op jit(solution)/shard_map/all_to_all | solution.py:163
  375.9 3.8 fusion.65
  381.0 32.2 %all-gather.17.cloned.1.call-done = bf16[1024,2048]{1,0:T(8,128)(2,1)} async-done(((bf16[128,2048]{1,0:T(8,128)(2,1)}), bf16[1024,2048]{1,0:T(8,128)(2,1)}) %all-gather.17.cloned.1.call-update) | async-done | bytes 4194320 | tf_op jit(solution)/shard_map/all_gather | solution.py:123
  413.2 4.0 fusion.40
  417.3 4.2 fusion.36
  421.6 14.7 %all_to_all.61 = bf16[8,128,352]{1,2,0:T(8,128)(2,1)S(1)} all-to-all(bf16[8,128,352]{1,2,0:T(8,128)(2,1)S(1)} %bitcast.179), channel_id=1, replica_groups=mesh['rep'=2,'fs'=16,'tp'=8] {'tp'}, dimensions={0} | all-to-all | bytes 1441792 | tf_op jit(solution)/shard_map/all_to_all | solution.py:128
  436.3 1.8 fusion.66
  (232 shorter events, 21.0 us)
Async XLA Ops:
  6.5 228.2 %copy-start = (bf16[2048,32]{0,1:T(8,128)(2,1)S(1)}, bf16[2048,32]{0,1:T(8,128)(2,1)}, u32[]{:S(2)}) copy-start(bf16[2048,32]{0,1:T(8,128)(2,1)} %param.24) | copy-start | bytes 393220
  6.5 126.1 %all-gather.7.cloned.1.call-start = ((), (), s32[]{:S(2)}) async-start(), calls=%async_computation.5 | async-start | bytes 3063808 | tf_op jit(solution)/shard_map/all_gather | solution.py:57
  10.4 113.2 %copy-start.13 = (f32[3,2048]{1,0:T(4,128)S(1)}, f32[3,2048]{1,0:T(4,128)}, u32[]{:S(2)}) copy-start(f32[3,2048]{1,0:T(4,128)} %param.29) | copy-start | bytes 73732
  10.4 47.3 %all-to-all-start.1 = ((bf16[16,352,128]{2,1,0:T(8,128)(2,1)}), bf16[16,352,128]{2,1,0:T(8,128)(2,1)S(1)}, u32[]{:S(2)}, u32[]{:S(2)}) async-start(bf16[16,352,128]{2,1,0:T(8,128)(2,1)} %broadcast_in_dim.32), calls=%async_computation.1 | async-start | bytes 2883584 | tf_op jit(solution)/shard_map/all_to_all | solution.py:40
  19.6 130.5 %all-gather.9.cloned.1.call-start = ((), (), s32[]{:S(2)}) async-start(), calls=%async_computation.6 | async-start | bytes 4718592 | tf_op jit(solution)/shard_map/all_gather | solution.py:123
  57.9 24.0 %collective-permute-start = (bf16[352,2048]{1,0:T(8,128)(2,1)S(1)}, bf16[352,2048]{1,0:T(8,128)(2,1)S(1)}, u32[]{:S(2)}, u32[]{:S(2)}) collective-permute-start(bf16[352,2048]{1,0:T(8,128)(2,1)S(1)} %copy_bitcast_fusion), channel_id=1, source_target_pairs={{0,1},{1,2},{2,3},{3,4},{4,5},{5,6},{6,7},{7,0},{8,9},{9,10},{10,1... | collective-permute-start | bytes 4325384 | tf_op jit(solution)/shard_map/ppermute | solution.py:29
  81.9 1.1 copy-start.6
  83.0 18.4 %collective-permute-start.1 = (bf16[352,2048]{1,0:T(8,128)(2,1)S(1)}, bf16[352,2048]{1,0:T(8,128)(2,1)S(1)}, u32[]{:S(2)}, u32[]{:S(2)}) collective-permute-start(bf16[352,2048]{1,0:T(8,128)(2,1)S(1)} %collective-permute-done), channel_id=1, source_target_pairs={{0,1},{1,2},{2,3},{3,4},{4,5},{5,6},{6,7},{7,0},{8,9},{9,10},{10,1... | collective-permute-start | bytes 4325384 | tf_op jit(solution)/shard_map/ppermute | solution.py:29
  85.5 19.6 %collective-permute-start.4 = (bf16[352,2048]{1,0:T(8,128)(2,1)S(1)}, bf16[352,2048]{1,0:T(8,128)(2,1)}, u32[]{:S(2)}, u32[]{:S(2)}) collective-permute-start(bf16[352,2048]{1,0:T(8,128)(2,1)S(1)} %copy_bitcast_fusion), channel_id=1, source_target_pairs={{1,0},{2,1},{3,2},{4,3},{5,4},{6,5},{7,6},{0,7},{9,8},{10,9},{11,1... | collective-permute-start | bytes 4325384 | tf_op jit(solution)/shard_map/ppermute | solution.py:31
  101.5 1.1 copy-start.8
  102.6 18.4 %collective-permute-start.2 = (bf16[352,2048]{1,0:T(8,128)(2,1)S(1)}, bf16[352,2048]{1,0:T(8,128)(2,1)}, u32[]{:S(2)}, u32[]{:S(2)}) collective-permute-start(bf16[352,2048]{1,0:T(8,128)(2,1)S(1)} %collective-permute-done.1), channel_id=1, source_target_pairs={{0,1},{1,2},{2,3},{3,4},{4,5},{5,6},{6,7},{7,0},{8,9},{9,10},{10,1... | collective-permute-start | bytes 4325384 | tf_op jit(solution)/shard_map/ppermute | solution.py:29
  105.0 19.8 %collective-permute-start.5 = (bf16[352,2048]{1,0:T(8,128)(2,1)}, bf16[352,2048]{1,0:T(8,128)(2,1)}, u32[]{:S(2)}, u32[]{:S(2)}) collective-permute-start(bf16[352,2048]{1,0:T(8,128)(2,1)} %collective-permute-done.4), channel_id=1, source_target_pairs={{1,0},{2,1},{3,2},{4,3},{5,4},{6,5},{7,6},{0,7},{9,8},{10,9},{11,1... | collective-permute-start | bytes 4325384 | tf_op jit(solution)/shard_map/ppermute | solution.py:31
  121.0 40.4 %collective-permute-start.3 = (bf16[352,2048]{1,0:T(8,128)(2,1)}, bf16[352,2048]{1,0:T(8,128)(2,1)}, u32[]{:S(2)}, u32[]{:S(2)}) collective-permute-start(bf16[352,2048]{1,0:T(8,128)(2,1)} %collective-permute-done.2), channel_id=1, source_target_pairs={{0,1},{1,2},{2,3},{3,4},{4,5},{5,6},{6,7},{7,0},{8,9},{9,10},{10,1... | collective-permute-start | bytes 4325384 | tf_op jit(solution)/shard_map/ppermute | solution.py:29
  124.9 51.0 %collective-permute-start.6 = (bf16[352,2048]{1,0:T(8,128)(2,1)}, bf16[352,2048]{1,0:T(8,128)(2,1)}, u32[]{:S(2)}, u32[]{:S(2)}) collective-permute-start(bf16[352,2048]{1,0:T(8,128)(2,1)} %collective-permute-done.5), channel_id=1, source_target_pairs={{1,0},{2,1},{3,2},{4,3},{5,4},{6,5},{7,6},{0,7},{9,8},{10,9},{11,1... | collective-permute-start | bytes 4325384 | tf_op jit(solution)/shard_map/ppermute | solution.py:31
  150.0 4.5 %copy-start.18 = (bf16[1024,2048]{1,0:T(8,128)(2,1)S(1)}, bf16[1024,2048]{1,0:T(8,128)(2,1)}, u32[]{:S(2)}) copy-start(bf16[1024,2048]{1,0:T(8,128)(2,1)} %all-gather.9.cloned.1.call-done) | copy-start | bytes 12582916
  150.0 4.8 %copy-start.19 = (bf16[2048,704]{0,1:T(8,128)(2,1)S(1)}, bf16[2048,704]{0,1:T(8,128)(2,1)}, u32[]{:S(2)}) copy-start(bf16[2048,704]{0,1:T(8,128)(2,1)} %all-gather.7.cloned.1.call-done) | copy-start | bytes 8650756
  157.7 31.2 %all-to-all-start = ((bf16[8,128,352]{1,2,0:T(8,128)(2,1)}), bf16[8,128,352]{1,2,0:T(8,128)(2,1)S(1)}, u32[]{:S(2)}, u32[]{:S(2)}) async-start(bf16[8,128,352]{1,2,0:T(8,128)(2,1)} %bitcast.142), calls=%async_computation | async-start | bytes 1441792 | tf_op jit(solution)/shard_map/all_to_all | solution.py:128
  161.4 73.3 %all-gather.11.cloned.1.call-start = ((), (), s32[]{:S(2)}) async-start(), calls=%async_computation.7 | async-start | bytes 4718592 | tf_op jit(solution)/shard_map/all_gather | solution.py:135
  161.4 5.6 %copy-start.9 = (bf16[352,2048]{1,0:T(8,128)(2,1)S(1)}, bf16[352,2048]{1,0:T(8,128)(2,1)}, u32[]{:S(2)}) copy-start(bf16[352,2048]{1,0:T(8,128)(2,1)} %copy-done.8) | copy-start | bytes 4325380
  164.2 4.0 copy-start.7
  178.5 10.4 %copy-start.5 = (bf16[128,2048]{1,0:T(8,128)(2,1)S(1)}, bf16[128,2048]{1,0:T(8,128)(2,1)}, u32[]{:S(2)}) copy-start(bf16[128,2048]{1,0:T(8,128)(2,1)} %param.16) | copy-start | bytes 1572868
  195.0 1.4 copy-start.14
  195.0 1.6 copy-start.15
  195.0 1.7 copy-start.10
  195.0 1.7 copy-start.11
  195.0 2.4 copy-start.12
  195.0 39.7 %copy-start.16 = (bf16[32,64]{1,0:T(8,128)(2,1)S(1)}, bf16[32,64]{1,0:T(8,128)(2,1)}, u32[]{:S(2)}) copy-start(bf16[32,64]{1,0:T(8,128)(2,1)} %param.25) | copy-start | bytes 12292
  195.0 39.7 %copy-start.17 = (f32[64]{0:T(128)S(1)}, f32[64]{0:T(128)}, u32[]{:S(2)}) copy-start(f32[64]{0:T(128)} %param.26) | copy-start | bytes 772
  196.4 110.5 %all-gather.13.cloned.1.call-start = ((), (), s32[]{:S(2)}) async-start(), calls=%async_computation.8 | async-start | bytes 1671168 | tf_op jit(solution)/shard_map/all_gather | solution.py:57
  198.5 22.7 %all-to-all-start.3 = ((bf16[16,128,128]{1,2,0:T(8,128)(2,1)}), bf16[16,128,128]{1,2,0:T(8,128)(2,1)S(1)}, u32[]{:S(2)}, u32[]{:S(2)}) async-start(bf16[16,128,128]{1,2,0:T(8,128)(2,1)} %broadcast_in_dim.35), calls=%async_computation.3 | async-start | bytes 1048576 | tf_op jit(solution)/shard_map/all_to_all | solution.py:40
  206.9 162.5 %all-gather.15.cloned.1.call-start = ((), (), s32[]{:S(2)}) async-start(), calls=%async_computation.9 | async-start | bytes 4718592 | tf_op jit(solution)/shard_map/all_gather | solution.py:162
  221.2 0.8 copy-start.4
  318.3 30.8 %copy-start.21 = (f32[128]{0:T(128)S(1)}, f32[128]{0:T(128)}, u32[]{:S(2)}) copy-start(f32[128]{0:T(128)} %param.27) | copy-start | bytes 1540
  349.2 26.7 %copy-start.2 = (bf16[128,2048]{1,0:T(8,128)(2,1)S(1)}, bf16[128,2048]{1,0:T(8,128)(2,1)}, u32[]{:S(2)}) copy-start(bf16[128,2048]{1,0:T(8,128)(2,1)} %multiply_convert_fusion.2) | copy-start | bytes 1572868
  353.7 22.2 %all-to-all-start.2 = ((bf16[8,128,128]{1,2,0:T(8,128)(2,1)}), bf16[8,128,128]{1,2,0:T(8,128)(2,1)S(1)}, u32[]{:S(2)}, u32[]{:S(2)}) async-start(bf16[8,128,128]{1,2,0:T(8,128)(2,1)} %copy.58), calls=%async_computation.2 | async-start | bytes 524288 | tf_op jit(solution)/shard_map/all_to_all | solution.py:163
  369.4 43.8 %all-gather.17.cloned.1.call-start = ((), (), s32[]{:S(2)}) async-start(), calls=%async_computation.10 | async-start | bytes 4718592 | tf_op jit(solution)/shard_map/all_gather | solution.py:123
  379.7 33.5 %copy-start.20 = (bf16[2048,704]{0,1:T(8,128)(2,1)S(1)}, bf16[2048,704]{0,1:T(8,128)(2,1)}, u32[]{:S(2)}) copy-start(bf16[2048,704]{0,1:T(8,128)(2,1)} %all-gather.7.cloned.1.call-done) | copy-start | bytes 8650756
  413.2 23.0 %slice-start = ((s8[11534336]{0:T(1024)(128)(4,1)}), s8[4194304]{0:T(1024)(128)(4,1)S(1)}, s32[]{:S(2)}) async-start(s8[11534336]{0:T(1024)(128)(4,1)} %bitcast.171), calls=%async_computation.11 | async-start | bytes 8388608
  413.2 23.0 %slice-start.1 = ((s8[11534336]{0:T(1024)(128)(4,1)}), s8[4194304]{0:T(1024)(128)(4,1)S(1)}, s32[]{:S(2)}) async-start(s8[11534336]{0:T(1024)(128)(4,1)} %bitcast.171), calls=%async_computation.12 | async-start | bytes 8388608
  417.2 19.0 %slice-start.2 = ((s8[11534336]{0:T(1024)(128)(4,1)}), s8[3145728]{0:T(1024)(128)(4,1)S(1)}, s32[]{:S(2)}) async-start(s8[11534336]{0:T(1024)(128)(4,1)} %bitcast.171), calls=%async_computation.13 | async-start | bytes 6291456
  421.4 14.8 %copy-start.3 = (bf16[128,2048]{1,0:T(8,128)(2,1)S(1)}, bf16[128,2048]{1,0:T(8,128)(2,1)}, u32[]{:S(2)}) copy-start(bf16[128,2048]{1,0:T(8,128)(2,1)} %multiply_convert_fusion.1) | copy-start | bytes 1572868
  436.3 3.1 copy-start.1
Sparse Core Ops, SparseCore 0:
  9.0 88.9 all-gather.6
  99.9 50.0 all-gather.8
  196.5 38.1 all-gather.10
  236.4 70.4 all-gather.12
  308.6 47.8 all-gather.14
  381.1 32.0 all-gather.16
